TPU v7x, 32 devices: a whole 2x2x4 slice. The times are simulated.
32 devices in a mesh: sp: 4 (over z), tp: 4 (over y, x), dp: 2 (over core).
Axes of the slice: x: 2, y: 2, z: 4, core: 2. Of those that a mesh axis runs over, the one named last changes fastest.
Arguments:
- latent: bfloat16 [8192, 2048], P(('dp', 'sp', 'tp')), parts along dimension 0, may hold values from -6 to 6
- cond: bfloat16 [4096], P('dp'), parts along dimension 0, may hold values from -6 to 6
- ctx_rows: bfloat16 [2048, 2048], P(('dp', 'sp')), parts along dimension 0, may hold values from -6 to 6
- ctx_cond: bfloat16 [2048], replicated, may hold values from -6 to 6
- mod_weight: bfloat16 [3, 2048, 2048], P(None, 'sp', 'tp'), may hold values from -0.125 to 0.125
- norm_gain: float32 [2048], replicated, may hold values from 0.1 to 1.9
- out_gain: float32 [2048], replicated, may hold values from 0.1 to 1.9
- w_query: bfloat16 [2048, 1024], replicated, may hold values from -16 to 16
- w_key: bfloat16 [2048, 256], replicated, may hold values from -1 to 1
- w_value: bfloat16 [2048, 256], replicated, may hold values from -0.125 to 0.125
- w_out: bfloat16 [1024, 2048], replicated, may hold values from -0.1875 to 0.1875
- sink: float32 [16], replicated, may hold values from 3 to 8
Outputs:
- updated: bfloat16 [8192, 2048], P(('dp', 'sp', 'tp')), parts along dimension 0
There are 2 independent parts, one for each index of `dp`. A program takes and returns all parts, laid end to end along the dimension named above; an argument that names none is the same for every part. Nothing has to cross between parts.
All inputs are finite; a program needn't handle non-finite values.
Results may differ from a plain program's by a relative error of at most 0.0053.
Values may be sent and summed in bfloat16 or wider, within the bound.
A program may use at most 128 MiB of HBM per device.

v0:
```python
import functools
import math

import jax
import jax.numpy as jnp
from jax import lax
from jax.experimental import pallas as pl
from jax.experimental.pallas import tpu as pltpu
from jax.sharding import PartitionSpec as P

HEAD_DIM = 64
WINDOW = 128
SPAN = 128
GRID_W = 64
EPSILON = 1e-06
NEG_BIG = -1e30
LANES = 128
MESH = pl.DeviceIdType.MESH
F32 = jnp.float32
BF16 = jnp.bfloat16


def dot(a, b):
    return jnp.dot(a, b, preferred_element_type=F32)


def dot_t(a, b):
    return lax.dot_general(a, b, (((1,), (1,)), ((), ())), preferred_element_type=F32)


def kernel(
    sp_n,
    tp_n,
    latent_hbm,
    cond_ref,
    ctx_hbm,
    ctx_cond_ref,
    mod_hbm,
    norm_gain_ref,
    out_gain_ref,
    wq_hbm,
    wk_hbm,
    wv_hbm,
    wo_hbm,
    sink_ref,
    out_ref,
    mod,
    ctx,
    wk,
    wv,
    latent,
    wq,
    wo,
    hidden,
    silu,
    parts,
    vecs,
    rms,
    table,
    bias,
    ctx_kv,
    own_kv,
    q_rot,
    q_plain,
    acc,
    tops,
    mixed,
    projected,
    load_sem,
    sum_send,
    sum_recv,
    gat_send,
    gat_recv,
    z_send,
    z_recv,
    f_send,
    f_recv,
    halo_send,
    halo_recv,
):
    sp = lax.axis_index("sp")
    tp = lax.axis_index("tp")
    me = sp * tp_n + tp
    way = 1 - 2 * ((2 * sp) // sp_n)
    count = sp_n * tp_n
    rows, width = latent.shape
    ctx_rows = ctx.shape[0]
    key_width = wk.shape[1]
    kv_width = 2 * key_width
    piece = mod.shape[1]
    cols = mod.shape[2]
    quarter = ctx_rows // tp_n
    blocks = rows // SPAN
    pairs = key_width // LANES
    heads = wq.shape[1] // HEAD_DIM
    group = heads // (key_width // HEAD_DIM)

    barrier = pltpu.get_barrier_semaphore()
    for step in range(1, count):
        other = lax.rem(me + step, count)
        pl.semaphore_signal(
            barrier,
            inc=1,
            device_id={"sp": other // tp_n, "tp": lax.rem(other, tp_n)},
            device_id_type=MESH,
        )

    loads = []
    for at, (source, target) in enumerate(
        ((mod_hbm, mod), (ctx_hbm, ctx), (wk_hbm, wk), (wv_hbm, wv), (latent_hbm, latent), (wq_hbm, wq), (wo_hbm, wo))
    ):
        load = pltpu.make_async_copy(source, target, load_sem.at[at])
        load.start()
        loads.append(load)

    own = []
    for which, ref in enumerate((cond_ref, ctx_cond_ref)):
        v = ref[...].astype(F32)
        silu[which] = v / (1.0 + jnp.exp(-v))
        tiles = [
            silu[which, pl.ds(sp * (piece // LANES) + i, 1)] for i in range(piece // LANES)
        ]
        own.append(jnp.broadcast_to(jnp.concatenate(tiles, axis=1), (16, piece)))
    row_id = lax.broadcasted_iota(jnp.int32, (16, piece), 0)
    loads[0].wait()
    total = None
    for which in range(3):
        left = jnp.where(
            row_id == 2 * which, own[0], jnp.where(row_id == 2 * which + 1, own[1], 0.0)
        ).astype(BF16)
        term = dot(left, mod[which])
        total = term if total is None else total + term
    parts[sp] = total[:8]
    pl.semaphore_wait(barrier, count - 1)

    def sum_copy(step, slot):
        return pltpu.make_async_remote_copy(
            src_ref=parts.at[sp],
            dst_ref=parts.at[slot],
            send_sem=sum_send.at[step - 1],
            recv_sem=sum_recv.at[slot],
            device_id={"sp": lax.rem(sp + step, sp_n), "tp": tp},
            device_id_type=MESH,
        )

    for step in range(1, sp_n):
        sum_copy(step, sp).start()

    def row_rms(ref, at):
        x = ref[...].astype(F32)
        mean = jnp.sum(x * x, axis=-1, keepdims=True) * (1.0 / width)
        rms[at, : ref.shape[0]] = jnp.broadcast_to(lax.rsqrt(mean + EPSILON), (ref.shape[0], LANES))

    loads[1].wait()
    row_rms(ctx, 1)

    for step in range(1, sp_n):
        sum_copy(step, lax.rem(sp + step, sp_n)).wait_recv()
    summed = parts[0]
    for s in range(1, sp_n):
        summed = summed + parts[s]
    vecs[tp] = summed

    def gat_copy(step, slot):
        return pltpu.make_async_remote_copy(
            src_ref=vecs.at[tp],
            dst_ref=vecs.at[slot],
            send_sem=gat_send.at[step - 1],
            recv_sem=gat_recv.at[slot],
            device_id={"sp": sp, "tp": lax.rem(tp + step, tp_n)},
            device_id_type=MESH,
        )

    for step in range(1, tp_n):
        gat_copy(step, tp).start()

    loads[4].wait()
    row_rms(latent, 0)

    lane = lax.broadcasted_iota(jnp.int32, (rows, LANES), 1)
    low_half = (lane & (HEAD_DIM // 2)) == 0
    position = me * rows + lax.broadcasted_iota(jnp.int32, (rows, LANES), 0)
    freqs = HEAD_DIM // 4
    slot = (lane & (freqs - 1)).astype(F32)
    coord = jnp.where((lane & freqs) == 0, position // GRID_W, position % GRID_W).astype(F32)
    angle = coord * jnp.exp(slot * (-math.log(10000.0) / freqs))
    table[0] = jnp.cos(angle)
    sine = jnp.sin(angle)
    table[1] = jnp.where(low_half, -sine, sine)
    q_at = lax.broadcasted_iota(jnp.int32, (SPAN, 3 * SPAN), 0)
    k_at = lax.broadcasted_iota(jnp.int32, (SPAN, 3 * SPAN), 1) - SPAN
    for b in range(blocks):
        k_pos = me * rows + b * SPAN + k_at
        ok = (jnp.abs(q_at - k_at) <= WINDOW) & (k_pos >= 0) & (k_pos < count * rows)
        bias[b] = jnp.where(ok, 0.0, NEG_BIG)

    for step in range(1, tp_n):
        gat_copy(step, lax.rem(tp + step, tp_n)).wait_recv()

    def modulate(ref, which):
        r = rms[which, : ref.shape[0]]
        r = jnp.concatenate([r] * (cols // LANES), axis=1)
        for t in range(tp_n):
            at = pl.ds(t * cols, cols)
            gain = norm_gain_ref[:, at] * (1.0 + vecs[t, 2 + which : 3 + which])
            shift = vecs[t, which : which + 1]
            hidden[: ref.shape[0], at] = (ref[:, at].astype(F32) * r * gain + shift).astype(BF16)

    modulate(ctx, 1)
    loads[2].wait()
    loads[3].wait()
    ctx_at = pl.ds(pl.multiple_of(sp * ctx_rows, 16), ctx_rows)
    ctx_kv[ctx_at, :key_width] = dot(hidden[:ctx_rows], wk[...]).astype(BF16)
    ctx_kv[ctx_at, key_width:] = dot(hidden[:ctx_rows], wv[...]).astype(BF16)

    def peer(step):
        return lax.rem(sp + way * step + sp_n, sp_n)

    def share(s, t):
        return ctx_kv.at[pl.ds(pl.multiple_of(s * ctx_rows + t * quarter, 16), quarter)]

    def z_copy(step, s):
        return pltpu.make_async_remote_copy(
            src_ref=share(s, tp),
            dst_ref=share(s, tp),
            send_sem=z_send.at[step - 1],
            recv_sem=z_recv.at[s],
            device_id={"sp": peer(step), "tp": tp},
            device_id_type=MESH,
        )

    def f_copy(far, step, s, t):
        return pltpu.make_async_remote_copy(
            src_ref=share(s, t),
            dst_ref=share(s, t),
            send_sem=f_send.at[(far - 1) * (tp_n - 1) + step - 1],
            recv_sem=f_recv.at[s * tp_n + t],
            device_id={"sp": sp, "tp": lax.rem(tp + step, tp_n)},
            device_id_type=MESH,
        )

    for step in range(1, sp_n):
        z_copy(step, sp).start()

    def rotate(x):
        swapped = jnp.where(
            low_half, pltpu.roll(x, LANES - HEAD_DIM // 2, 1), pltpu.roll(x, HEAD_DIM // 2, 1)
        )
        return x * table[0] + swapped * table[1]

    modulate(latent, 0)
    keys = dot(hidden[:rows], wk[...]).astype(BF16).astype(F32)
    for p in range(pairs):
        at = slice(p * LANES, (p + 1) * LANES)
        own_kv[SPAN : SPAN + rows, at] = rotate(keys[:, at]).astype(BF16)
    own_kv[SPAN : SPAN + rows, key_width:] = dot(hidden[:rows], wv[...]).astype(BF16)

    after = lax.rem(me + 1, count)
    before = lax.rem(me + count - 1, count)
    to_next = pltpu.make_async_remote_copy(
        src_ref=own_kv.at[pl.ds(rows, SPAN)],
        dst_ref=own_kv.at[pl.ds(0, SPAN)],
        send_sem=halo_send.at[0],
        recv_sem=halo_recv.at[0],
        device_id={"sp": after // tp_n, "tp": lax.rem(after, tp_n)},
        device_id_type=MESH,
    )
    to_prev = pltpu.make_async_remote_copy(
        src_ref=own_kv.at[pl.ds(SPAN, SPAN)],
        dst_ref=own_kv.at[pl.ds(SPAN + rows, SPAN)],
        send_sem=halo_send.at[1],
        recv_sem=halo_recv.at[1],
        device_id={"sp": before // tp_n, "tp": lax.rem(before, tp_n)},
        device_id_type=MESH,
    )

    @pl.when(me < count - 1)
    def _():
        to_next.start()

    @pl.when(me > 0)
    def _():
        to_prev.start()

    @pl.when(me == 0)
    def _():
        own_kv[:SPAN] = jnp.zeros((SPAN, kv_width), BF16)

    @pl.when(me == count - 1)
    def _():
        own_kv[SPAN + rows :] = jnp.zeros((SPAN, kv_width), BF16)

    in_low = lane < HEAD_DIM
    loads[5].wait()
    tile = group * HEAD_DIM
    for kv in range(heads // group):
        q = dot(hidden[:rows], wq[:, kv * tile : (kv + 1) * tile]).astype(BF16).astype(F32)
        q = q * (HEAD_DIM**-0.5)
        keep = in_low if kv % 2 == 0 else jnp.logical_not(in_low)
        for j in range(tile // LANES):
            plain = q[:, j * LANES : (j + 1) * LANES]
            for target, x in ((q_plain, plain), (q_rot, rotate(plain))):
                turned = pltpu.roll(x, HEAD_DIM, 1)
                first, second = (x, turned) if kv % 2 == 0 else (turned, x)
                h = kv * group + 2 * j
                target[h] = jnp.where(keep, first, 0.0).astype(BF16)
                target[h + 1] = jnp.where(keep, second, 0.0).astype(BF16)

    kv_heads = heads // group
    per = -(-(sp_n - 1) // kv_heads)

    def lanes_of(kv):
        pair = kv // 2
        return (
            pl.ds(pl.multiple_of(pair * LANES, LANES), LANES),
            pl.ds(pl.multiple_of(key_width + pair * LANES, LANES), LANES),
        )

    def with_ones(v):
        return jnp.concatenate([v, jnp.ones(v.shape, BF16)], axis=1)

    def forward(far):
        s = peer(far)
        z_copy(far, s).wait_recv()
        for step in range(1, tp_n):
            f_copy(far, step, s, tp).start()

    def own_block(kv, carry):
        for i in range(per):
            far = kv * per + i + 1

            @pl.when(far < sp_n)
            def _():
                forward(far)

        k_lanes, v_lanes = lanes_of(kv)
        k = ctx_kv[ctx_at, k_lanes]
        v = with_ones(ctx_kv[ctx_at, v_lanes])
        for g in range(group):
            h = kv * group + g
            scores = dot_t(q_plain[h], k)
            sink = sink_ref[h]
            top = jnp.maximum(jnp.max(scores, axis=-1, keepdims=True), sink)
            weights = jnp.exp(scores - top).astype(BF16)
            term = dot(weights, v)
            acc[h, :, :LANES] = term[:, :LANES]
            acc[h, :, LANES:] = term[:, LANES:] + jnp.exp(sink - top)
            tops[h] = jnp.broadcast_to(top, (rows, LANES))
        return carry

    lax.fori_loop(0, kv_heads, own_block, 0)

    def update(h, at, old, top, term):
        decay = jnp.exp(old - top)
        acc[h, at, :LANES] = acc[h, at, :LANES] * decay + term[:, :LANES]
        acc[h, at, LANES:] = acc[h, at, LANES:] * decay + term[:, LANES:]
        tops[h, at] = top

    @pl.when(me > 0)
    def _():
        to_next.wait_recv()

    @pl.when(me < count - 1)
    def _():
        to_prev.wait_recv()

    def window(kv, carry):
        k_lanes, v_lanes = lanes_of(kv)
        for b in range(blocks):
            at = pl.ds(b * SPAN, SPAN)
            band = pl.ds(b * SPAN, 3 * SPAN)
            k = own_kv[band, k_lanes]
            v = with_ones(own_kv[band, v_lanes])
            for g in range(group):
                h = kv * group + g
                scores = dot_t(q_rot[h, at], k) + bias[b]
                old = tops[h, at]
                top = jnp.maximum(old, jnp.max(scores, axis=-1, keepdims=True))
                weights = jnp.exp(scores - jnp.concatenate([top] * 3, axis=1)).astype(BF16)
                update(h, at, old, top, dot(weights, v))
        return carry

    lax.fori_loop(0, kv_heads, window, 0)

    def far_block(far, carry):
        s = peer(far)
        for step in range(1, tp_n):
            f_copy(far, step, s, lax.rem(tp + step, tp_n)).wait_recv()
        block = pl.ds(pl.multiple_of(s * ctx_rows, 16), ctx_rows)

        def one(kv, inner):
            k_lanes, v_lanes = lanes_of(kv)
            k = ctx_kv[block, k_lanes]
            v = with_ones(ctx_kv[block, v_lanes])
            for g in range(group):
                h = kv * group + g
                scores = dot_t(q_plain[h], k)
                old = tops[h]
                top = jnp.maximum(old, jnp.max(scores, axis=-1, keepdims=True))
                weights = jnp.exp(scores - top[:, :1]).astype(BF16)
                update(h, pl.ds(0, rows), old, top, dot(weights, v))
            return inner

        return lax.fori_loop(0, kv_heads, one, carry)

    lax.fori_loop(1, sp_n, far_block, 0)

    half_tiles = tile // LANES
    for lane_tile in range(heads // 2):
        out = []
        for h in (2 * lane_tile, 2 * lane_tile + 1):
            out.append(acc[h, :, :LANES] / acc[h, :, LANES:])
        if (lane_tile // half_tiles) % 2 == 0:
            both = jnp.where(in_low, out[0], pltpu.roll(out[1], HEAD_DIM, 1))
        else:
            both = jnp.where(in_low, pltpu.roll(out[0], HEAD_DIM, 1), out[1])
        mixed[:, lane_tile * LANES : (lane_tile + 1) * LANES] = both.astype(BF16)

    loads[6].wait()
    wide = 256

    def project(at, squares):
        lanes = pl.ds(pl.multiple_of(at * wide, wide), wide)
        y = dot(mixed[...], wo[:, lanes])
        projected[:, lanes] = y
        return squares + jnp.sum(y * y, axis=-1, keepdims=True)

    squares = lax.fori_loop(0, width // wide, project, jnp.zeros((rows, 1), F32))
    r = lax.rsqrt(squares * (1.0 / width) + EPSILON)
    for t in range(tp_n):
        at = pl.ds(t * cols, cols)
        gain = vecs[t, 4:5] * out_gain_ref[:, at]
        out_ref[:, at] = (latent[:, at].astype(F32) + projected[:, at] * r * gain).astype(BF16)

    for step in range(1, sp_n):
        sum_copy(step, sp).wait_send()
        z_copy(step, sp).wait_send()
    for step in range(1, tp_n):
        gat_copy(step, tp).wait_send()
        for far in range(1, sp_n):
            s = peer(far)
            f_copy(far, step, s, tp).wait_send()

    @pl.when(me < count - 1)
    def _():
        to_next.wait_send()

    @pl.when(me > 0)
    def _():
        to_prev.wait_send()


def solution(mesh):
    sp_n, tp_n = mesh.shape["sp"], mesh.shape["tp"]

    def shards(
        latent, cond, ctx_rows, ctx_cond, mod_weight, norm_gain, out_gain, w_query, w_key, w_value, w_out, sink
    ):
        rows, width = latent.shape
        context = ctx_rows.shape[0]
        key_width = w_key.shape[1]
        heads = w_query.shape[1] // HEAD_DIM
        cols = mod_weight.shape[2]
        any_spec = pl.BlockSpec(memory_space=pl.ANY)
        vmem = pl.BlockSpec(memory_space=pltpu.VMEM)
        dma = pltpu.SemaphoreType.DMA
        return pl.pallas_call(
            functools.partial(kernel, sp_n, tp_n),
            out_shape=jax.ShapeDtypeStruct((rows, width), BF16),
            in_specs=[
                any_spec,
                vmem,
                any_spec,
                vmem,
                any_spec,
                vmem,
                vmem,
                any_spec,
                any_spec,
                any_spec,
                any_spec,
                pl.BlockSpec(memory_space=pltpu.SMEM),
            ],
            out_specs=vmem,
            scratch_shapes=[
                pltpu.VMEM(mod_weight.shape, BF16),
                pltpu.VMEM(ctx_rows.shape, BF16),
                pltpu.VMEM(w_key.shape, BF16),
                pltpu.VMEM(w_value.shape, BF16),
                pltpu.VMEM(latent.shape, BF16),
                pltpu.VMEM(w_query.shape, BF16),
                pltpu.VMEM(w_out.shape, BF16),
                pltpu.VMEM((max(rows, context), width), BF16),
                pltpu.VMEM((2, width // LANES, LANES), F32),
                pltpu.VMEM((sp_n, 8, cols), F32),
                pltpu.VMEM((tp_n, 8, cols), F32),
                pltpu.VMEM((2, max(rows, context), LANES), F32),
                pltpu.VMEM((2, rows, LANES), F32),
                pltpu.VMEM((rows // SPAN, SPAN, 3 * SPAN), F32),
                pltpu.VMEM((sp_n * context, 2 * key_width), BF16),
                pltpu.VMEM((rows + 2 * SPAN, 2 * key_width), BF16),
                pltpu.VMEM((heads, rows, LANES), BF16),
                pltpu.VMEM((heads, rows, LANES), BF16),
                pltpu.VMEM((heads, rows, 2 * LANES), F32),
                pltpu.VMEM((heads, rows, LANES), F32),
                pltpu.VMEM((rows, heads * HEAD_DIM), BF16),
                pltpu.VMEM((rows, width), F32),
                dma((7,)),
                dma((sp_n - 1,)),
                dma((sp_n,)),
                dma((tp_n - 1,)),
                dma((tp_n,)),
                dma((sp_n - 1,)),
                dma((sp_n,)),
                dma(((sp_n - 1) * (tp_n - 1),)),
                dma((sp_n * tp_n,)),
                dma((2,)),
                dma((2,)),
            ],
            compiler_params=pltpu.CompilerParams(
                collective_id=0, has_side_effects=True, vmem_limit_bytes=60 * 1024 * 1024
            ),
        )(
            latent,
            cond.reshape(-1, LANES),
            ctx_rows,
            ctx_cond.reshape(-1, LANES),
            mod_weight,
            norm_gain.reshape(1, -1),
            out_gain.reshape(1, -1),
            w_query,
            w_key,
            w_value,
            w_out,
            sink,
        )

    placed = (
        P(("dp", "sp", "tp"), None),
        P("dp"),
        P(("dp", "sp"), None),
        P(),
        P(None, "sp", "tp"),
        P(),
        P(),
        P(),
        P(),
        P(),
        P(),
        P(),
    )
    return jax.shard_map(
        shards, mesh=mesh, in_specs=placed, out_specs=P(("dp", "sp", "tp"), None), check_vma=False
    )
```

profile of v0, /device:TPU:0, one launch (start us, length us, event | category | flops | bytes accessed | tf_op | source)
XLA Modules:
  0.0 46.2 jit_solution(9363339375888113130)
XLA Ops:
  0.0 43.9 %shard_map.118 = bf16[256,2048]{1,0:T(8,128)(2,1)} custom-call(bf16[256,2048]{1,0:T(8,128)(2,1)} %latent_hbm.1, bf16[16,128]{1,0:T(8,128)(2,1)} %bitcast.6, bf16[256,2048]{1,0:T(8,128)(2,1)} %ctx_hbm.1, bf16[16,128]{1,0:T(8,128)(2,1)} %bitcast.7, bf16[3,512,512]{2,1,0:T(8,128)(2,1)} %mod_hbm.1, f32[1,2048]{1,0:T(1,128)} %bitcast.4, f32[1,2048]{1,0:T(1,128)} %bitcast.5, ...), custom_call_target="tpu_custom_call" | custom-call | tf_op jit(solution)/shard_map/pallas_call | solution.py:467
  43.9 2.3 %copy.14 = bf16[256,2048]{1,0:T(8,128)(2,1)} copy(bf16[256,2048]{1,0:T(8,128)(2,1)} %shard_map.118) | data formatting | bytes 2097152
where the time goes:
time: 46.4 us; the launch traced here: 46.2 us
  Pallas kernels  43.9 us (95%)
  local copies, waits for them, and re-layouts  2.3 us (5%)
    pallas_call x1, Pallas kernels, shards(): pl.pallas_call(functools.partial(kernel, sp_n, tp_n), out_shape=jax.Shape...  43.9 us
    unnamed x1, local copies, waits for them, and re-layouts  2.3 us

commit v1 on v0

--- a/solution.py
+++ b/solution.py
@@ -46,12 +46,12 @@
     out_ref,
     mod,
     ctx,
-    wk,
-    wv,
+    wkv,
     latent,
     wq,
     wo,
     hidden,
+    ctx_hidden,
     silu,
     parts,
     vecs,
@@ -60,6 +60,11 @@
     bias,
     ctx_kv,
     own_kv,
+    table_t,
+    own_val,
+    ctx_val,
+    scores,
+    weights,
     q_rot,
     q_plain,
     acc,
@@ -85,8 +90,8 @@
     count = sp_n * tp_n
     rows, width = latent.shape
     ctx_rows = ctx.shape[0]
-    key_width = wk.shape[1]
-    kv_width = 2 * key_width
+    kv_width = wkv.shape[1]
+    key_width = kv_width // 2
     piece = mod.shape[1]
     cols = mod.shape[2]
     quarter = ctx_rows // tp_n
@@ -107,7 +112,7 @@
 
     loads = []
     for at, (source, target) in enumerate(
-        ((mod_hbm, mod), (ctx_hbm, ctx), (wk_hbm, wk), (wv_hbm, wv), (latent_hbm, latent), (wq_hbm, wq), (wo_hbm, wo))
+        ((mod_hbm, mod), (ctx_hbm, ctx), (wk_hbm, wkv.at[:, :key_width]), (wv_hbm, wkv.at[:, key_width:]), (latent_hbm, latent), (wq_hbm, wq), (wo_hbm, wo))
     ):
         load = pltpu.make_async_copy(source, target, load_sem.at[at])
         load.start()
@@ -187,31 +192,51 @@
     table[0] = jnp.cos(angle)
     sine = jnp.sin(angle)
     table[1] = jnp.where(low_half, -sine, sine)
-    q_at = lax.broadcasted_iota(jnp.int32, (SPAN, 3 * SPAN), 0)
-    k_at = lax.broadcasted_iota(jnp.int32, (SPAN, 3 * SPAN), 1) - SPAN
+    half = HEAD_DIM // 2
+    row_t = lax.broadcasted_iota(jnp.int32, (half, rows), 0)
+    pos_t = me * rows + lax.broadcasted_iota(jnp.int32, (half, rows), 1)
+    slot_t = (row_t & (freqs - 1)).astype(F32)
+    coord_t = jnp.where((row_t & freqs) == 0, pos_t // GRID_W, pos_t % GRID_W).astype(F32)
+    angle_t = coord_t * jnp.exp(slot_t * (-math.log(10000.0) / freqs))
+    table_t[0] = jnp.cos(angle_t)
+    table_t[1] = jnp.sin(angle_t)
+    k_at = lax.broadcasted_iota(jnp.int32, (SPAN, SPAN), 0)
+    q_at = lax.broadcasted_iota(jnp.int32, (SPAN, SPAN), 1)
     for b in range(blocks):
-        k_pos = me * rows + b * SPAN + k_at
-        ok = (jnp.abs(q_at - k_at) <= WINDOW) & (k_pos >= 0) & (k_pos < count * rows)
-        bias[b] = jnp.where(ok, 0.0, NEG_BIG)
+        for side, shift in ((0, -SPAN), (1, SPAN)):
+            k_pos = me * rows + b * SPAN + k_at + shift
+            ok = (jnp.abs(q_at - k_at - shift) <= WINDOW) & (k_pos >= 0) & (k_pos < count * rows)
+            bias[b, side] = jnp.where(ok, 0.0, NEG_BIG)
+    own_val[:, HEAD_DIM:] = jnp.ones((own_val.shape[0], own_val.shape[1] - HEAD_DIM, own_val.shape[2]), BF16)
+    ctx_val[:, :, HEAD_DIM:] = jnp.ones(
+        (sp_n, ctx_val.shape[1], ctx_val.shape[2] - HEAD_DIM, ctx_rows), BF16
+    )
+    q_rot[...] = jnp.zeros_like(q_rot)
+    q_plain[...] = jnp.zeros_like(q_plain)
 
     for step in range(1, tp_n):
         gat_copy(step, lax.rem(tp + step, tp_n)).wait_recv()
 
-    def modulate(ref, which):
-        r = rms[which, : ref.shape[0]]
+    def modulate(ref, target, which, first, size):
+        at_rows = pl.ds(first, size)
+        r = rms[which, at_rows]
         r = jnp.concatenate([r] * (cols // LANES), axis=1)
         for t in range(tp_n):
             at = pl.ds(t * cols, cols)
             gain = norm_gain_ref[:, at] * (1.0 + vecs[t, 2 + which : 3 + which])
             shift = vecs[t, which : which + 1]
-            hidden[: ref.shape[0], at] = (ref[:, at].astype(F32) * r * gain + shift).astype(BF16)
-
-    modulate(ctx, 1)
+            target[at_rows, at] = (ref[at_rows, at].astype(F32) * r * gain + shift).astype(BF16)
+
+    def ctx_part(t):
+        first = pl.multiple_of(t * quarter, 16)
+        modulate(ctx, ctx_hidden, 1, first, quarter)
+        at = pl.ds(pl.multiple_of(sp * ctx_rows + t * quarter, 16), quarter)
+        ctx_kv[at] = dot(ctx_hidden[pl.ds(first, quarter)], wkv[...]).astype(BF16)
+
+    ctx_at = pl.ds(pl.multiple_of(sp * ctx_rows, 16), ctx_rows)
     loads[2].wait()
     loads[3].wait()
-    ctx_at = pl.ds(pl.multiple_of(sp * ctx_rows, 16), ctx_rows)
-    ctx_kv[ctx_at, :key_width] = dot(hidden[:ctx_rows], wk[...]).astype(BF16)
-    ctx_kv[ctx_at, key_width:] = dot(hidden[:ctx_rows], wv[...]).astype(BF16)
+    ctx_part(tp)
 
     def peer(step):
         return lax.rem(sp + way * step + sp_n, sp_n)
@@ -248,12 +273,12 @@
         )
         return x * table[0] + swapped * table[1]
 
-    modulate(latent, 0)
-    keys = dot(hidden[:rows], wk[...]).astype(BF16).astype(F32)
+    modulate(latent, hidden, 0, 0, rows)
+    kv = dot(hidden[...], wkv[...]).astype(BF16)
     for p in range(pairs):
         at = slice(p * LANES, (p + 1) * LANES)
-        own_kv[SPAN : SPAN + rows, at] = rotate(keys[:, at]).astype(BF16)
-    own_kv[SPAN : SPAN + rows, key_width:] = dot(hidden[:rows], wv[...]).astype(BF16)
+        own_kv[SPAN : SPAN + rows, at] = rotate(kv[:, at].astype(F32)).astype(BF16)
+    own_kv[SPAN : SPAN + rows, key_width:] = kv[:, key_width:]
 
     after = lax.rem(me + 1, count)
     before = lax.rem(me + count - 1, count)
@@ -290,34 +315,8 @@
     def _():
         own_kv[SPAN + rows :] = jnp.zeros((SPAN, kv_width), BF16)
 
-    in_low = lane < HEAD_DIM
-    loads[5].wait()
+    kv_heads = heads // group
     tile = group * HEAD_DIM
-    for kv in range(heads // group):
-        q = dot(hidden[:rows], wq[:, kv * tile : (kv + 1) * tile]).astype(BF16).astype(F32)
-        q = q * (HEAD_DIM**-0.5)
-        keep = in_low if kv % 2 == 0 else jnp.logical_not(in_low)
-        for j in range(tile // LANES):
-            plain = q[:, j * LANES : (j + 1) * LANES]
-            for target, x in ((q_plain, plain), (q_rot, rotate(plain))):
-                turned = pltpu.roll(x, HEAD_DIM, 1)
-                first, second = (x, turned) if kv % 2 == 0 else (turned, x)
-                h = kv * group + 2 * j
-                target[h] = jnp.where(keep, first, 0.0).astype(BF16)
-                target[h + 1] = jnp.where(keep, second, 0.0).astype(BF16)
-
-    kv_heads = heads // group
-    per = -(-(sp_n - 1) // kv_heads)
-
-    def lanes_of(kv):
-        pair = kv // 2
-        return (
-            pl.ds(pl.multiple_of(pair * LANES, LANES), LANES),
-            pl.ds(pl.multiple_of(key_width + pair * LANES, LANES), LANES),
-        )
-
-    def with_ones(v):
-        return jnp.concatenate([v, jnp.ones(v.shape, BF16)], axis=1)
 
     def forward(far):
         s = peer(far)
@@ -325,107 +324,195 @@
         for step in range(1, tp_n):
             f_copy(far, step, s, tp).start()
 
-    def own_block(kv, carry):
-        for i in range(per):
-            far = kv * per + i + 1
-
-            @pl.when(far < sp_n)
-            def _():
-                forward(far)
-
-        k_lanes, v_lanes = lanes_of(kv)
-        k = ctx_kv[ctx_at, k_lanes]
-        v = with_ones(ctx_kv[ctx_at, v_lanes])
+    loads[5].wait()
+    cos_t, sin_t = table_t[0], table_t[1]
+    for kv in range(kv_heads):
+        q = dot(hidden[...], wq[:, kv * tile : (kv + 1) * tile]) * (HEAD_DIM**-0.5)
+        q_t = jnp.transpose(q.astype(BF16)).astype(F32)
+        base = (kv % 2) * HEAD_DIM
         for g in range(group):
             h = kv * group + g
-            scores = dot_t(q_plain[h], k)
-            sink = sink_ref[h]
-            top = jnp.maximum(jnp.max(scores, axis=-1, keepdims=True), sink)
-            weights = jnp.exp(scores - top).astype(BF16)
-            term = dot(weights, v)
-            acc[h, :, :LANES] = term[:, :LANES]
-            acc[h, :, LANES:] = term[:, LANES:] + jnp.exp(sink - top)
-            tops[h] = jnp.broadcast_to(top, (rows, LANES))
-        return carry
-
-    lax.fori_loop(0, kv_heads, own_block, 0)
-
-    def update(h, at, old, top, term):
-        decay = jnp.exp(old - top)
-        acc[h, at, :LANES] = acc[h, at, :LANES] * decay + term[:, :LANES]
-        acc[h, at, LANES:] = acc[h, at, LANES:] * decay + term[:, LANES:]
-        tops[h, at] = top
-
-    @pl.when(me > 0)
-    def _():
-        to_next.wait_recv()
-
-    @pl.when(me < count - 1)
-    def _():
-        to_prev.wait_recv()
-
-    def window(kv, carry):
-        k_lanes, v_lanes = lanes_of(kv)
-        for b in range(blocks):
-            at = pl.ds(b * SPAN, SPAN)
-            band = pl.ds(b * SPAN, 3 * SPAN)
-            k = own_kv[band, k_lanes]
-            v = with_ones(own_kv[band, v_lanes])
-            for g in range(group):
-                h = kv * group + g
-                scores = dot_t(q_rot[h, at], k) + bias[b]
-                old = tops[h, at]
-                top = jnp.maximum(old, jnp.max(scores, axis=-1, keepdims=True))
-                weights = jnp.exp(scores - jnp.concatenate([top] * 3, axis=1)).astype(BF16)
-                update(h, at, old, top, dot(weights, v))
-        return carry
-
-    lax.fori_loop(0, kv_heads, window, 0)
-
-    def far_block(far, carry):
+            x1 = q_t[g * HEAD_DIM : g * HEAD_DIM + half]
+            x2 = q_t[g * HEAD_DIM + half : (g + 1) * HEAD_DIM]
+            q_plain[h, base : base + half] = x1.astype(BF16)
+            q_plain[h, base + half : base + HEAD_DIM] = x2.astype(BF16)
+            r1 = (x1 * cos_t - x2 * sin_t).astype(BF16)
+            r2 = (x1 * sin_t + x2 * cos_t).astype(BF16)
+            side = slice(g * SPAN, (g + 1) * SPAN)
+            for b in range(blocks):
+                i = kv * blocks + b
+                q_rot[i, base : base + half, side] = r1[:, b * SPAN : (b + 1) * SPAN]
+                q_rot[i, base + half : base + HEAD_DIM, side] = r2[:, b * SPAN : (b + 1) * SPAN]
+
+    for step in range(1, tp_n):
+        ctx_part(lax.rem(tp + step, tp_n))
+    forward(1)
+
+    def turn(source, at, target):
+        for p in range(pairs):
+            v_t = jnp.transpose(source[at, key_width + p * LANES : key_width + (p + 1) * LANES])
+            target[2 * p, :HEAD_DIM] = v_t[:HEAD_DIM]
+            target[2 * p + 1, :HEAD_DIM] = v_t[HEAD_DIM:]
+
+    def key_lanes(kv):
+        return slice(kv // 2 * LANES, (kv // 2 + 1) * LANES)
+
+    def state(ref, parts):
+        return jnp.concatenate([ref[h, :, at] for h, at in parts], axis=1)
+
+    def unit(parts, keys, query, bands, value, first):
+        wide = sum(at.stop - at.start for _, at in parts)
+        memo = {}
+
+        def score(buf):
+            k = keys()
+            s = dot(k, query())
+            if bands is not None:
+                low, high = (jnp.concatenate([bias[bands, i]] * (wide // SPAN), axis=1) for i in range(2))
+                s = jnp.concatenate([s[:SPAN] + low, s[SPAN : 2 * SPAN], s[2 * SPAN :] + high], axis=0)
+            memo["size"] = s.shape[0]
+            scores[buf, : s.shape[0], :wide] = s
+            memo["most"] = jnp.max(s, axis=0, keepdims=True)
+
+        def soften(buf):
+            s = scores[buf, : memo["size"], :wide]
+            if first:
+                old = jnp.concatenate([jnp.full((1, at.stop - at.start), sink_ref[h], F32) for h, at in parts], axis=1)
+            else:
+                old = state(tops, parts)
+            top = jnp.maximum(old, memo["most"])
+            weights[buf, : memo["size"], :wide] = jnp.exp(s - top).astype(BF16)
+            memo["decay"] = jnp.exp(old - top)
+            col = 0
+            for h, at in parts:
+                size = at.stop - at.start
+                tops[h, :, at] = top[:, col : col + size]
+                col += size
+
+        def mix(buf):
+            term = dot(value(), weights[buf, : memo["size"], :wide])
+            decay = memo["decay"]
+            col = 0
+            for h, at in parts:
+                size = at.stop - at.start
+                here = slice(col, col + size)
+                if first:
+                    acc[h, :HEAD_DIM, at] = term[:HEAD_DIM, here]
+                    acc[h, HEAD_DIM:, at] = term[HEAD_DIM:, here] + decay[:, here]
+                else:
+                    acc[h, :, at] = acc[h, :, at] * decay[:, here] + term[:, here]
+                col += size
+
+        return score, soften, mix
+
+    def context_units(at, slot, first):
+        units = []
+        for pair in range(heads // 2):
+            kv = 2 * pair // group
+            units.append(
+                unit(
+                    [(2 * pair, slice(0, rows)), (2 * pair + 1, slice(0, rows))],
+                    lambda kv=kv: ctx_kv[at, key_lanes(kv)],
+                    lambda pair=pair: jnp.concatenate([q_plain[2 * pair], q_plain[2 * pair + 1]], axis=1),
+                    None,
+                    lambda kv=kv: ctx_val[slot, kv],
+                    first,
+                )
+            )
+        return units
+
+    def window_units():
+        units = []
+        for kv in range(kv_heads):
+            for b in range(blocks):
+                band = slice(b * SPAN, (b + 3) * SPAN)
+                units.append(
+                    unit(
+                        [(kv * group + g, slice(b * SPAN, (b + 1) * SPAN)) for g in range(group)],
+                        lambda kv=kv, band=band: own_kv[band, key_lanes(kv)],
+                        lambda kv=kv, b=b: q_rot[kv * blocks + b],
+                        b,
+                        lambda kv=kv, band=band: own_val[kv, :, band],
+                        False,
+                    )
+                )
+        return units
+
+    def run(units, before):
+        for i in range(len(units) + 2):
+            if i in before:
+                before[i]()
+            if i < len(units):
+                units[i][0](i % 2)
+            if 0 <= i - 1 < len(units):
+                units[i - 1][1]((i - 1) % 2)
+            if 0 <= i - 2 < len(units):
+                units[i - 2][2](i % 2)
+
+    def halo():
+        @pl.when(me > 0)
+        def _():
+            to_next.wait_recv()
+
+        @pl.when(me < count - 1)
+        def _():
+            to_prev.wait_recv()
+
+        turn(own_kv, slice(None), own_val)
+
+    def arrive(far):
         s = peer(far)
         for step in range(1, tp_n):
-            f_copy(far, step, s, lax.rem(tp + step, tp_n)).wait_recv()
-        block = pl.ds(pl.multiple_of(s * ctx_rows, 16), ctx_rows)
-
-        def one(kv, inner):
-            k_lanes, v_lanes = lanes_of(kv)
-            k = ctx_kv[block, k_lanes]
-            v = with_ones(ctx_kv[block, v_lanes])
-            for g in range(group):
-                h = kv * group + g
-                scores = dot_t(q_plain[h], k)
-                old = tops[h]
-                top = jnp.maximum(old, jnp.max(scores, axis=-1, keepdims=True))
-                weights = jnp.exp(scores - top[:, :1]).astype(BF16)
-                update(h, pl.ds(0, rows), old, top, dot(weights, v))
-            return inner
-
-        return lax.fori_loop(0, kv_heads, one, carry)
-
-    lax.fori_loop(1, sp_n, far_block, 0)
-
-    half_tiles = tile // LANES
-    for lane_tile in range(heads // 2):
-        out = []
-        for h in (2 * lane_tile, 2 * lane_tile + 1):
-            out.append(acc[h, :, :LANES] / acc[h, :, LANES:])
-        if (lane_tile // half_tiles) % 2 == 0:
-            both = jnp.where(in_low, out[0], pltpu.roll(out[1], HEAD_DIM, 1))
-        else:
-            both = jnp.where(in_low, pltpu.roll(out[0], HEAD_DIM, 1), out[1])
-        mixed[:, lane_tile * LANES : (lane_tile + 1) * LANES] = both.astype(BF16)
+          f_copy(far, step, s, lax.rem(tp + step, tp_n)).wait_recv()
+        at = pl.ds(pl.multiple_of(s * ctx_rows, 16), ctx_rows)
+        turn(ctx_kv, at, ctx_val.at[far])
+        return at
+
+    turn(ctx_kv, ctx_at, ctx_val.at[0])
+    units = context_units(ctx_at, 0, True)
+    after_own = len(units)
+    units += window_units()
+
+    def second():
+        if sp_n > 2:
+            forward(2)
+        halo()
+
+    run(units, {after_own: second})
+    for far in range(3, sp_n):
+        forward(far)
+
+    if sp_n <= 4:
+        units, before = [], {}
+        for far in range(1, sp_n):
+            before[len(units)] = functools.partial(arrive, far)
+            at = pl.ds(pl.multiple_of(peer(far) * ctx_rows, 16), ctx_rows)
+            units += context_units(at, far, False)
+        run(units, before)
+    else:
+
+        def far_block(far, carry):
+            run(context_units(arrive(far), far, False), {})
+            return carry
+
+        lax.fori_loop(1, sp_n, far_block, 0)
+
+    for pair in range(heads // 2):
+        both = []
+        for h in (2 * pair, 2 * pair + 1):
+            both.append(acc[h, :HEAD_DIM] * (1.0 / acc[h, HEAD_DIM : HEAD_DIM + 1]))
+        both = jnp.concatenate(both, axis=0).astype(BF16)
+        mixed[:, pair * LANES : (pair + 1) * LANES] = jnp.transpose(both)
 
     loads[6].wait()
     wide = 256
-
-    def project(at, squares):
-        lanes = pl.ds(pl.multiple_of(at * wide, wide), wide)
+    squares = jnp.zeros((rows, 1), F32)
+    for at in range(width // wide):
+        lanes = slice(at * wide, (at + 1) * wide)
         y = dot(mixed[...], wo[:, lanes])
         projected[:, lanes] = y
-        return squares + jnp.sum(y * y, axis=-1, keepdims=True)
-
-    squares = lax.fori_loop(0, width // wide, project, jnp.zeros((rows, 1), F32))
+        squares = squares + jnp.sum(y * y, axis=-1, keepdims=True)
+
     r = lax.rsqrt(squares * (1.0 / width) + EPSILON)
     for t in range(tp_n):
         at = pl.ds(t * cols, cols)
@@ -460,6 +547,7 @@
         context = ctx_rows.shape[0]
         key_width = w_key.shape[1]
         heads = w_query.shape[1] // HEAD_DIM
+        kv_heads = key_width // HEAD_DIM
         cols = mod_weight.shape[2]
         any_spec = pl.BlockSpec(memory_space=pl.ANY)
         vmem = pl.BlockSpec(memory_space=pltpu.VMEM)
@@ -485,24 +573,29 @@
             scratch_shapes=[
                 pltpu.VMEM(mod_weight.shape, BF16),
                 pltpu.VMEM(ctx_rows.shape, BF16),
-                pltpu.VMEM(w_key.shape, BF16),
-                pltpu.VMEM(w_value.shape, BF16),
+                pltpu.VMEM((width, 2 * key_width), BF16),
                 pltpu.VMEM(latent.shape, BF16),
                 pltpu.VMEM(w_query.shape, BF16),
                 pltpu.VMEM(w_out.shape, BF16),
-                pltpu.VMEM((max(rows, context), width), BF16),
+                pltpu.VMEM((rows, width), BF16),
+                pltpu.VMEM((context, width), BF16),
                 pltpu.VMEM((2, width // LANES, LANES), F32),
                 pltpu.VMEM((sp_n, 8, cols), F32),
                 pltpu.VMEM((tp_n, 8, cols), F32),
                 pltpu.VMEM((2, max(rows, context), LANES), F32),
                 pltpu.VMEM((2, rows, LANES), F32),
-                pltpu.VMEM((rows // SPAN, SPAN, 3 * SPAN), F32),
+                pltpu.VMEM((rows // SPAN, 2, SPAN, SPAN), F32),
                 pltpu.VMEM((sp_n * context, 2 * key_width), BF16),
                 pltpu.VMEM((rows + 2 * SPAN, 2 * key_width), BF16),
-                pltpu.VMEM((heads, rows, LANES), BF16),
-                pltpu.VMEM((heads, rows, LANES), BF16),
-                pltpu.VMEM((heads, rows, 2 * LANES), F32),
-                pltpu.VMEM((heads, rows, LANES), F32),
+                pltpu.VMEM((2, HEAD_DIM // 2, rows), F32),
+                pltpu.VMEM((kv_heads, HEAD_DIM + 16, rows + 2 * SPAN), BF16),
+                pltpu.VMEM((sp_n, kv_heads, HEAD_DIM + 16, context), BF16),
+                pltpu.VMEM((2, max(3 * SPAN, context), max(2 * rows, heads // kv_heads * SPAN)), F32),
+                pltpu.VMEM((2, max(3 * SPAN, context), max(2 * rows, heads // kv_heads * SPAN)), BF16),
+                pltpu.VMEM((kv_heads * (rows // SPAN), LANES, heads // kv_heads * SPAN), BF16),
+                pltpu.VMEM((heads, LANES, rows), BF16),
+                pltpu.VMEM((heads, HEAD_DIM + 16, rows), F32),
+                pltpu.VMEM((heads, 1, rows), F32),
                 pltpu.VMEM((rows, heads * HEAD_DIM), BF16),
                 pltpu.VMEM((rows, width), F32),
                 dma((7,)),
@@ -518,9 +611,9 @@
                 dma((2,)),
             ],
             compiler_params=pltpu.CompilerParams(
-                collective_id=0, has_side_effects=True, vmem_limit_bytes=60 * 1024 * 1024
+                collective_id=0, has_side_effects=True, vmem_limit_bytes=50 * 1024 * 1024
             ),
-        )(
+        )(*[pltpu.with_memory_space_constraint(a, pltpu.HBM) for a in (
             latent,
             cond.reshape(-1, LANES),
             ctx_rows,
@@ -533,7 +626,7 @@
             w_value,
             w_out,
             sink,
-        )
+        )])
 
     placed = (
         P(("dp", "sp", "tp"), None),

time: 46.4 us -> 35 us (0.75)
  Pallas kernels: 43.9 us -> 33.9 us
  local copies, waits for them, and re-layouts: 2.3 us -> 0.97 us
    pallas_call x1, Pallas kernels: 43.9 us -> 33.9 us  [shards(): pl.pallas_call(functools.partial(kernel, sp_n, tp_n), out_shape=jax.Shape...]
    unnamed x1, local copies, waits for them, and re-layouts: 2.3 us -> 0.97 us
where the time goes in v1:
time: 35 us; the launch traced here: 34.9 us
  Pallas kernels  33.9 us (97%)
  local copies, waits for them, and re-layouts  0.97 us (3%)
    pallas_call x1, Pallas kernels, shards(): pl.pallas_call(functools.partial(kernel, sp_n, tp_n), out_shape=jax.Shape...  33.9 us
    unnamed x1, local copies, waits for them, and re-layouts  0.97 us

profile of v1, /device:TPU:0, one launch (start us, length us, event | category | flops | bytes accessed | tf_op | source)
XLA Modules:
  0.0 34.9 jit_solution(17610295330596353181)
XLA Ops:
  0.0 33.9 %shard_map.118 = bf16[256,2048]{1,0:T(8,128)(2,1)S(1)} custom-call(bf16[256,2048]{1,0:T(8,128)(2,1)} %latent_hbm.1, bf16[16,128]{1,0:T(8,128)(2,1)} %bitcast.6, bf16[256,2048]{1,0:T(8,128)(2,1)} %ctx_hbm.1, bf16[16,128]{1,0:T(8,128)(2,1)} %bitcast.7, bf16[3,512,512]{2,1,0:T(8,128)(2,1)} %mod_hbm.1, f32[1,2048]{1,0:T(1,128)} %bitcast.4, f32[1,2048]{1,0:T(1,128)} %bitcast.5, ...), custom_call_target="tpu_custom_call" | custom-call | tf_op jit(solution)/shard_map/pallas_call | solution.py:555
  33.9 1.0 %copy.14 = bf16[256,2048]{1,0:T(8,128)(2,1)} copy(bf16[256,2048]{1,0:T(8,128)(2,1)S(1)} %shard_map.118) | data formatting | bytes 2097152

commit v2 on v1

--- a/solution.py
+++ b/solution.py
@@ -15,6 +15,7 @@
 EPSILON = 1e-06
 NEG_BIG = -1e30
 LANES = 128
+LOG2E = math.log2(math.e)
 MESH = pl.DeviceIdType.MESH
 F32 = jnp.float32
 BF16 = jnp.bfloat16
@@ -22,28 +23,30 @@
 
 def dot(a, b):
     return jnp.dot(a, b, preferred_element_type=F32)
-
-
-def dot_t(a, b):
-    return lax.dot_general(a, b, (((1,), (1,)), ((), ())), preferred_element_type=F32)
 
 
 def kernel(
     sp_n,
     tp_n,
     latent_hbm,
-    cond_ref,
+    cond_hbm,
     ctx_hbm,
-    ctx_cond_ref,
+    ctx_cond_hbm,
     mod_hbm,
-    norm_gain_ref,
-    out_gain_ref,
+    norm_gain_hbm,
+    out_gain_hbm,
     wq_hbm,
     wk_hbm,
     wv_hbm,
     wo_hbm,
+    sink_hbm,
+    out_ref,
+    cond_ref,
+    ctx_cond_ref,
+    norm_gain_ref,
+    out_gain_ref,
     sink_ref,
-    out_ref,
+    small_sem,
     mod,
     ctx,
     wkv,
@@ -55,10 +58,13 @@
     silu,
     parts,
     vecs,
+    gate_parts,
+    gates,
     rms,
     table,
     bias,
     ctx_kv,
+    mine,
     own_kv,
     table_t,
     own_val,
@@ -72,6 +78,9 @@
     mixed,
     projected,
     load_sem,
+    gate_sem,
+    gate_gat_sem,
+    extra_sem,
     sum_send,
     sum_recv,
     gat_send,
@@ -87,6 +96,8 @@
     tp = lax.axis_index("tp")
     me = sp * tp_n + tp
     way = 1 - 2 * ((2 * sp) // sp_n)
+    rich = sp_n == 4 and tp_n == 4
+    inner = ((sp + 1) // 2) % 2 if rich else 0 * sp
     count = sp_n * tp_n
     rows, width = latent.shape
     ctx_rows = ctx.shape[0]
@@ -100,24 +111,72 @@
     heads = wq.shape[1] // HEAD_DIM
     group = heads // (key_width // HEAD_DIM)
 
+    after = lax.rem(me + 1, count)
+    before = lax.rem(me + count - 1, count)
+
+    def partner(step):
+        if rich:
+            return (tp + 1 - 2 * (tp % 2), tp + 2 - 4 * (tp // 2), 3 - tp)[step - 1]
+        return lax.rem(tp + step, tp_n)
+
     barrier = pltpu.get_barrier_semaphore()
-    for step in range(1, count):
-        other = lax.rem(me + step, count)
-        pl.semaphore_signal(
-            barrier,
-            inc=1,
-            device_id={"sp": other // tp_n, "tp": lax.rem(other, tp_n)},
-            device_id_type=MESH,
-        )
-
+
+    def greet(s, t):
+        pl.semaphore_signal(barrier, inc=1, device_id={"sp": s, "tp": t}, device_id_type=MESH)
+
+    for step in range(1, sp_n):
+        greet(lax.rem(sp + step, sp_n), tp)
+    for step in range(1, tp_n):
+        greet(sp, lax.rem(tp + step, tp_n))
+
+    cross_next = (tp + 1) // tp_n * (1 - (sp + 1) // sp_n)
+    cross_prev = (1 - (tp + tp_n - 1) // tp_n) * ((sp + sp_n - 1) // sp_n)
+
+    @pl.when(cross_next == 1)
+    def _():
+        greet(after // tp_n, lax.rem(after, tp_n))
+
+    @pl.when(cross_prev == 1)
+    def _():
+        greet(before // tp_n, lax.rem(before, tp_n))
+
+    small = [
+        pltpu.make_async_copy(source, target, small_sem.at[at])
+        for at, (source, target) in enumerate(
+            (
+                (cond_hbm, cond_ref),
+                (ctx_cond_hbm, ctx_cond_ref),
+                (norm_gain_hbm, norm_gain_ref),
+                (out_gain_hbm, out_gain_ref),
+                (sink_hbm, sink_ref),
+            )
+        )
+    ]
+    for load in small[:2]:
+        load.start()
+    mod_loads = []
+    for which in range(3):
+        load = pltpu.make_async_copy(mod_hbm.at[which], mod.at[which], load_sem.at[6 + which])
+        load.start()
+        mod_loads.append(load)
+    for load in small[2:]:
+        load.start()
     loads = []
     for at, (source, target) in enumerate(
-        ((mod_hbm, mod), (ctx_hbm, ctx), (wk_hbm, wkv.at[:, :key_width]), (wv_hbm, wkv.at[:, key_width:]), (latent_hbm, latent), (wq_hbm, wq), (wo_hbm, wo))
+        (
+            (ctx_hbm, ctx),
+            (latent_hbm, latent),
+            (wk_hbm, wkv.at[:, :key_width]),
+            (wv_hbm, wkv.at[:, key_width:]),
+            (wq_hbm, wq),
+            (wo_hbm, wo),
+        )
     ):
-        load = pltpu.make_async_copy(source, target, load_sem.at[at])
-        load.start()
-        loads.append(load)
-
+        loads.append(pltpu.make_async_copy(source, target, load_sem.at[at]))
+    ctx_load, latent_load, key_load, value_load, query_load, out_load = loads
+
+    small[0].wait()
+    small[1].wait()
     own = []
     for which, ref in enumerate((cond_ref, ctx_cond_ref)):
         v = ref[...].astype(F32)
@@ -127,16 +186,26 @@
         ]
         own.append(jnp.broadcast_to(jnp.concatenate(tiles, axis=1), (16, piece)))
     row_id = lax.broadcasted_iota(jnp.int32, (16, piece), 0)
-    loads[0].wait()
     total = None
     for which in range(3):
         left = jnp.where(
             row_id == 2 * which, own[0], jnp.where(row_id == 2 * which + 1, own[1], 0.0)
         ).astype(BF16)
+        mod_loads[which].wait()
         term = dot(left, mod[which])
-        total = term if total is None else total + term
-    parts[sp] = total[:8]
-    pl.semaphore_wait(barrier, count - 1)
+        if which < 2:
+            total = term if total is None else total + term
+        else:
+            gate = term[4:5]
+    fold = cols // 2
+    parts[sp] = jnp.concatenate([total[:4, :fold], total[:4, fold:]], axis=0)
+    gate_rows = cols // LANES
+    gate_parts[sp, :gate_rows] = jnp.concatenate(
+        [gate[:, i * LANES : (i + 1) * LANES] for i in range(gate_rows)], axis=0
+    )
+    for load in loads:
+        load.start()
+    pl.semaphore_wait(barrier, sp_n + tp_n - 2 + cross_next + cross_prev)
 
     def sum_copy(step, slot):
         return pltpu.make_async_remote_copy(
@@ -148,15 +217,37 @@
             device_id_type=MESH,
         )
 
+    def gate_sum_copy(step, slot):
+        return pltpu.make_async_remote_copy(
+            src_ref=gate_parts.at[sp],
+            dst_ref=gate_parts.at[slot],
+            send_sem=gate_sem.at[step - 1],
+            recv_sem=gate_sem.at[sp_n - 1 + slot],
+            device_id={"sp": lax.rem(sp + step, sp_n), "tp": tp},
+            device_id_type=MESH,
+        )
+
+    def gate_copy(step, slot):
+        return pltpu.make_async_remote_copy(
+            src_ref=gates.at[tp],
+            dst_ref=gates.at[slot],
+            send_sem=gate_gat_sem.at[step - 1],
+            recv_sem=gate_gat_sem.at[tp_n - 1 + slot],
+            device_id={"sp": sp, "tp": lax.rem(tp + step, tp_n)},
+            device_id_type=MESH,
+        )
+
     for step in range(1, sp_n):
         sum_copy(step, sp).start()
+    for step in range(1, sp_n):
+        gate_sum_copy(step, sp).start()
 
     def row_rms(ref, at):
         x = ref[...].astype(F32)
         mean = jnp.sum(x * x, axis=-1, keepdims=True) * (1.0 / width)
         rms[at, : ref.shape[0]] = jnp.broadcast_to(lax.rsqrt(mean + EPSILON), (ref.shape[0], LANES))
 
-    loads[1].wait()
+    ctx_load.wait()
     row_rms(ctx, 1)
 
     for step in range(1, sp_n):
@@ -172,14 +263,14 @@
             dst_ref=vecs.at[slot],
             send_sem=gat_send.at[step - 1],
             recv_sem=gat_recv.at[slot],
-            device_id={"sp": sp, "tp": lax.rem(tp + step, tp_n)},
+            device_id={"sp": sp, "tp": partner(step)},
             device_id_type=MESH,
         )
 
     for step in range(1, tp_n):
         gat_copy(step, tp).start()
 
-    loads[4].wait()
+    latent_load.wait()
     row_rms(latent, 0)
 
     lane = lax.broadcasted_iota(jnp.int32, (rows, LANES), 1)
@@ -214,31 +305,39 @@
     q_rot[...] = jnp.zeros_like(q_rot)
     q_plain[...] = jnp.zeros_like(q_plain)
 
-    for step in range(1, tp_n):
-        gat_copy(step, lax.rem(tp + step, tp_n)).wait_recv()
-
-    def modulate(ref, target, which, first, size):
+    def modulate(ref, target, which, first, size, t):
         at_rows = pl.ds(first, size)
         r = rms[which, at_rows]
-        r = jnp.concatenate([r] * (cols // LANES), axis=1)
-        for t in range(tp_n):
-            at = pl.ds(t * cols, cols)
-            gain = norm_gain_ref[:, at] * (1.0 + vecs[t, 2 + which : 3 + which])
-            shift = vecs[t, which : which + 1]
+        r = jnp.concatenate([r] * (fold // LANES), axis=1)
+        for i in range(2):
+            at = pl.ds(pl.multiple_of(t * cols + i * fold, LANES), fold)
+            low = 4 * i + which
+            gain = norm_gain_ref[:, at] * (1.0 + vecs[t, low + 2 : low + 3])
+            shift = vecs[t, low : low + 1]
             target[at_rows, at] = (ref[at_rows, at].astype(F32) * r * gain + shift).astype(BF16)
 
-    def ctx_part(t):
-        first = pl.multiple_of(t * quarter, 16)
-        modulate(ctx, ctx_hidden, 1, first, quarter)
-        at = pl.ds(pl.multiple_of(sp * ctx_rows + t * quarter, 16), quarter)
-        ctx_kv[at] = dot(ctx_hidden[pl.ds(first, quarter)], wkv[...]).astype(BF16)
-
-    ctx_at = pl.ds(pl.multiple_of(sp * ctx_rows, 16), ctx_rows)
-    loads[2].wait()
-    loads[3].wait()
-    ctx_part(tp)
+    def ctx_rows_of(t):
+        return pl.ds(pl.multiple_of(sp * ctx_rows + t * quarter, 16), quarter)
+
+    for load in small[2:]:
+        load.wait()
+    key_load.wait()
+    value_load.wait()
+    first = pl.multiple_of(tp * quarter, 16)
+    total = None
+    for step in range(tp_n):
+        t = tp if step == 0 else partner(step)
+        if step > 0:
+            gat_copy(step, t).wait_recv()
+        modulate(ctx, ctx_hidden, 1, first, quarter, t)
+        features = pl.ds(pl.multiple_of(t * cols, LANES), cols)
+        term = dot(ctx_hidden[pl.ds(first, quarter), features], wkv[features])
+        total = term if total is None else total + term
+    ctx_kv[ctx_rows_of(tp)] = total.astype(BF16)
 
     def peer(step):
+        if rich:
+            step = (1, 2 + inner, 3 - inner)[step - 1]
         return lax.rem(sp + way * step + sp_n, sp_n)
 
     def share(s, t):
@@ -254,34 +353,50 @@
             device_id_type=MESH,
         )
 
-    def f_copy(far, step, s, t):
+    def f_copy(far, step, s, t, back=False):
+        sent = tp_n - step if back and not rich else step
         return pltpu.make_async_remote_copy(
             src_ref=share(s, t),
             dst_ref=share(s, t),
             send_sem=f_send.at[(far - 1) * (tp_n - 1) + step - 1],
-            recv_sem=f_recv.at[s * tp_n + t],
-            device_id={"sp": sp, "tp": lax.rem(tp + step, tp_n)},
+            recv_sem=f_recv.at[(far - 1) * (tp_n - 1) + sent - 1],
+            device_id={"sp": sp, "tp": partner(step)},
             device_id_type=MESH,
         )
 
-    for step in range(1, sp_n):
-        z_copy(step, sp).start()
-
-    def rotate(x):
+    def extra_copy(step, s):
+        return pltpu.make_async_remote_copy(
+            src_ref=mine.at[pl.ds(pl.multiple_of(partner(3) * quarter, 16), quarter)],
+            dst_ref=share(s, partner(3)),
+            send_sem=extra_sem.at[step - 1],
+            recv_sem=extra_sem.at[2 + s],
+            device_id={"sp": peer(step), "tp": tp},
+            device_id_type=MESH,
+        )
+
+    def is_inner(run):
+        pl.when(inner == 1)(run)
+
+    def is_outer(run):
+        pl.when(inner == 0)(run)
+
+    if rich:
+        z_copy(1, sp).start()
+
+        @is_inner
+        def _():
+            z_copy(2, sp).start()
+            z_copy(3, sp).start()
+    else:
+        for step in range(1, sp_n):
+            z_copy(step, sp).start()
+
+    def rotate(x, at):
         swapped = jnp.where(
-            low_half, pltpu.roll(x, LANES - HEAD_DIM // 2, 1), pltpu.roll(x, HEAD_DIM // 2, 1)
-        )
-        return x * table[0] + swapped * table[1]
-
-    modulate(latent, hidden, 0, 0, rows)
-    kv = dot(hidden[...], wkv[...]).astype(BF16)
-    for p in range(pairs):
-        at = slice(p * LANES, (p + 1) * LANES)
-        own_kv[SPAN : SPAN + rows, at] = rotate(kv[:, at].astype(F32)).astype(BF16)
-    own_kv[SPAN : SPAN + rows, key_width:] = kv[:, key_width:]
-
-    after = lax.rem(me + 1, count)
-    before = lax.rem(me + count - 1, count)
+            low_half[at], pltpu.roll(x, LANES - HEAD_DIM // 2, 1), pltpu.roll(x, HEAD_DIM // 2, 1)
+        )
+        return x * table[0, at] + swapped * table[1, at]
+
     to_next = pltpu.make_async_remote_copy(
         src_ref=own_kv.at[pl.ds(rows, SPAN)],
         dst_ref=own_kv.at[pl.ds(0, SPAN)],
@@ -299,13 +414,32 @@
         device_id_type=MESH,
     )
 
+    for b in range(blocks):
+        at_rows = slice(b * SPAN, (b + 1) * SPAN)
+        for t in range(tp_n):
+            modulate(latent, hidden, 0, b * SPAN, SPAN, t)
+        kv = dot(hidden[at_rows], wkv[...]).astype(BF16)
+        to = slice((b + 1) * SPAN, (b + 2) * SPAN)
+        for p in range(pairs):
+            at = slice(p * LANES, (p + 1) * LANES)
+            own_kv[to, at] = rotate(kv[:, at].astype(F32), at_rows).astype(BF16)
+        own_kv[to, key_width:] = kv[:, key_width:]
+        if b == 0:
+
+            @pl.when(me > 0)
+            def _():
+                to_prev.start()
+
     @pl.when(me < count - 1)
     def _():
         to_next.start()
 
-    @pl.when(me > 0)
-    def _():
-        to_prev.start()
+    if rich:
+
+        @is_outer
+        def _():
+            z_copy(3, sp).start()
+            z_copy(2, sp).start()
 
     @pl.when(me == 0)
     def _():
@@ -321,13 +455,33 @@
     def forward(far):
         s = peer(far)
         z_copy(far, s).wait_recv()
-        for step in range(1, tp_n):
+        if not rich:
+            for step in range(1, tp_n):
+                f_copy(far, step, s, tp).start()
+            return
+        if far == 2:
+
+            @is_outer
+            def _():
+                f_copy(far, 3, s, tp).start()
+        elif far == 3:
+            f_copy(far, 3, s, tp).start()
+        for step in (1, 2):
             f_copy(far, step, s, tp).start()
 
-    loads[5].wait()
+    for step in range(1, sp_n):
+        gate_sum_copy(step, lax.rem(sp + step, sp_n)).wait_recv()
+    gate_total = gate_parts[0]
+    for i in range(1, sp_n):
+        gate_total = gate_total + gate_parts[i]
+    gates[tp] = gate_total
+    for step in range(1, tp_n):
+        gate_copy(step, tp).start()
+
+    query_load.wait()
     cos_t, sin_t = table_t[0], table_t[1]
     for kv in range(kv_heads):
-        q = dot(hidden[...], wq[:, kv * tile : (kv + 1) * tile]) * (HEAD_DIM**-0.5)
+        q = dot(hidden[...], wq[:, kv * tile : (kv + 1) * tile]) * (HEAD_DIM**-0.5 * LOG2E)
         q_t = jnp.transpose(q.astype(BF16)).astype(F32)
         base = (kv % 2) * HEAD_DIM
         for g in range(group):
@@ -345,8 +499,15 @@
                 q_rot[i, base + half : base + HEAD_DIM, side] = r2[:, b * SPAN : (b + 1) * SPAN]
 
     for step in range(1, tp_n):
-        ctx_part(lax.rem(tp + step, tp_n))
+        for t in range(tp_n):
+            modulate(ctx, ctx_hidden, 1, pl.multiple_of(partner(step) * quarter, 16), quarter, t)
+    mine[...] = dot(ctx_hidden[...], wkv[...]).astype(BF16)
+    if rich:
+        extra_copy(1, sp).start()
+        is_inner(lambda: extra_copy(2, sp).start())
     forward(1)
+    if rich:
+        is_inner(lambda: forward(2))
 
     def turn(source, at, target):
         for p in range(pairs):
@@ -377,12 +538,12 @@
         def soften(buf):
             s = scores[buf, : memo["size"], :wide]
             if first:
-                old = jnp.concatenate([jnp.full((1, at.stop - at.start), sink_ref[h], F32) for h, at in parts], axis=1)
+                old = jnp.concatenate([jnp.full((1, at.stop - at.start), sink_ref[h] * LOG2E, F32) for h, at in parts], axis=1)
             else:
                 old = state(tops, parts)
             top = jnp.maximum(old, memo["most"])
-            weights[buf, : memo["size"], :wide] = jnp.exp(s - top).astype(BF16)
-            memo["decay"] = jnp.exp(old - top)
+            weights[buf, : memo["size"], :wide] = jnp.exp2(s - top).astype(BF16)
+            memo["decay"] = jnp.exp2(old - top)
             col = 0
             for h, at in parts:
                 size = at.stop - at.start
@@ -405,14 +566,14 @@
 
         return score, soften, mix
 
-    def context_units(at, slot, first):
+    def context_units(source, at, slot, first):
         units = []
         for pair in range(heads // 2):
             kv = 2 * pair // group
             units.append(
                 unit(
                     [(2 * pair, slice(0, rows)), (2 * pair + 1, slice(0, rows))],
-                    lambda kv=kv: ctx_kv[at, key_lanes(kv)],
+                    lambda kv=kv: source[at, key_lanes(kv)],
                     lambda pair=pair: jnp.concatenate([q_plain[2 * pair], q_plain[2 * pair + 1]], axis=1),
                     None,
                     lambda kv=kv: ctx_val[slot, kv],
@@ -462,37 +623,56 @@
 
     def arrive(far):
         s = peer(far)
-        for step in range(1, tp_n):
-          f_copy(far, step, s, lax.rem(tp + step, tp_n)).wait_recv()
+        if rich:
+            for step in (1, 2):
+                f_copy(far, step, s, partner(step), True).wait_recv()
+            if far == 1:
+                extra_copy(far, s).wait_recv()
+            elif far == 2:
+                is_inner(lambda: extra_copy(far, s).wait_recv())
+                is_outer(lambda: f_copy(far, 3, s, partner(3), True).wait_recv())
+            else:
+                f_copy(far, 3, s, partner(3), True).wait_recv()
+        else:
+            for step in range(1, tp_n):
+                f_copy(far, step, s, partner(step), True).wait_recv()
         at = pl.ds(pl.multiple_of(s * ctx_rows, 16), ctx_rows)
         turn(ctx_kv, at, ctx_val.at[far])
         return at
 
-    turn(ctx_kv, ctx_at, ctx_val.at[0])
-    units = context_units(ctx_at, 0, True)
-    after_own = len(units)
+    turn(mine, slice(None), ctx_val.at[0])
+    units, hooks = context_units(mine, slice(None), 0, True), {}
+
+    def remote_units(far):
+        at = pl.ds(pl.multiple_of(peer(far) * ctx_rows, 16), ctx_rows)
+        return context_units(ctx_kv, at, far, False)
+
+    near = len(units)
     units += window_units()
 
-    def second():
-        if sp_n > 2:
-            forward(2)
+    def relay():
+        if rich:
+            is_outer(lambda: forward(2))
+            forward(3)
         halo()
 
-    run(units, {after_own: second})
-    for far in range(3, sp_n):
-        forward(far)
-
-    if sp_n <= 4:
-        units, before = [], {}
+    hooks[near] = relay
+    if rich:
         for far in range(1, sp_n):
-            before[len(units)] = functools.partial(arrive, far)
-            at = pl.ds(pl.multiple_of(peer(far) * ctx_rows, 16), ctx_rows)
-            units += context_units(at, far, False)
-        run(units, before)
+
+            def ready(far=far):
+                arrive(far)
+
+            hooks[len(units)] = ready
+            units += remote_units(far)
+        run(units, hooks)
     else:
+        run(units, hooks)
+        for far in range(2, sp_n):
+            forward(far)
 
         def far_block(far, carry):
-            run(context_units(arrive(far), far, False), {})
+            run(context_units(ctx_kv, arrive(far), far, False), {})
             return carry
 
         lax.fori_loop(1, sp_n, far_block, 0)
@@ -504,29 +684,43 @@
         both = jnp.concatenate(both, axis=0).astype(BF16)
         mixed[:, pair * LANES : (pair + 1) * LANES] = jnp.transpose(both)
 
-    loads[6].wait()
+    out_load.wait()
     wide = 256
-    squares = jnp.zeros((rows, 1), F32)
+    squares = jnp.zeros((rows, LANES), F32)
     for at in range(width // wide):
         lanes = slice(at * wide, (at + 1) * wide)
         y = dot(mixed[...], wo[:, lanes])
         projected[:, lanes] = y
-        squares = squares + jnp.sum(y * y, axis=-1, keepdims=True)
-
+        for i in range(wide // LANES):
+            part = y[:, i * LANES : (i + 1) * LANES]
+            squares = squares + part * part
+
+    for step in range(1, tp_n):
+        gate_copy(step, lax.rem(tp + step, tp_n)).wait_recv()
+    squares = jnp.sum(squares, axis=-1, keepdims=True)
     r = lax.rsqrt(squares * (1.0 / width) + EPSILON)
     for t in range(tp_n):
         at = pl.ds(t * cols, cols)
-        gain = vecs[t, 4:5] * out_gain_ref[:, at]
+        gate = jnp.concatenate([gates[t, i : i + 1] for i in range(gate_rows)], axis=1)
+        gain = gate * out_gain_ref[:, at]
         out_ref[:, at] = (latent[:, at].astype(F32) + projected[:, at] * r * gain).astype(BF16)
 
     for step in range(1, sp_n):
         sum_copy(step, sp).wait_send()
+        gate_sum_copy(step, sp).wait_send()
         z_copy(step, sp).wait_send()
     for step in range(1, tp_n):
         gat_copy(step, tp).wait_send()
+        gate_copy(step, tp).wait_send()
         for far in range(1, sp_n):
-            s = peer(far)
-            f_copy(far, step, s, tp).wait_send()
+            done = f_copy(far, step, peer(far), tp)
+            if not rich or step < 3 or far == 3:
+                done.wait_send()
+            elif far == 2:
+                is_outer(done.wait_send)
+    if rich:
+        extra_copy(1, sp).wait_send()
+        is_inner(lambda: extra_copy(2, sp).wait_send())
 
     @pl.when(me < count - 1)
     def _():
@@ -555,22 +749,15 @@
         return pl.pallas_call(
             functools.partial(kernel, sp_n, tp_n),
             out_shape=jax.ShapeDtypeStruct((rows, width), BF16),
-            in_specs=[
-                any_spec,
-                vmem,
-                any_spec,
-                vmem,
-                any_spec,
-                vmem,
-                vmem,
-                any_spec,
-                any_spec,
-                any_spec,
-                any_spec,
-                pl.BlockSpec(memory_space=pltpu.SMEM),
-            ],
+            in_specs=[any_spec] * 12,
             out_specs=vmem,
             scratch_shapes=[
+                pltpu.VMEM((width // LANES, LANES), BF16),
+                pltpu.VMEM((width // LANES, LANES), BF16),
+                pltpu.VMEM((1, width), F32),
+                pltpu.VMEM((1, width), F32),
+                pltpu.SMEM(sink.shape, F32),
+                dma((5,)),
                 pltpu.VMEM(mod_weight.shape, BF16),
                 pltpu.VMEM(ctx_rows.shape, BF16),
                 pltpu.VMEM((width, 2 * key_width), BF16),
@@ -580,12 +767,15 @@
                 pltpu.VMEM((rows, width), BF16),
                 pltpu.VMEM((context, width), BF16),
                 pltpu.VMEM((2, width // LANES, LANES), F32),
-                pltpu.VMEM((sp_n, 8, cols), F32),
-                pltpu.VMEM((tp_n, 8, cols), F32),
+                pltpu.VMEM((sp_n, 8, cols // 2), F32),
+                pltpu.VMEM((tp_n, 8, cols // 2), F32),
+                pltpu.VMEM((sp_n, cols // LANES, LANES), F32),
+                pltpu.VMEM((tp_n, cols // LANES, LANES), F32),
                 pltpu.VMEM((2, max(rows, context), LANES), F32),
                 pltpu.VMEM((2, rows, LANES), F32),
                 pltpu.VMEM((rows // SPAN, 2, SPAN, SPAN), F32),
                 pltpu.VMEM((sp_n * context, 2 * key_width), BF16),
+                pltpu.VMEM((context, 2 * key_width), BF16),
                 pltpu.VMEM((rows + 2 * SPAN, 2 * key_width), BF16),
                 pltpu.VMEM((2, HEAD_DIM // 2, rows), F32),
                 pltpu.VMEM((kv_heads, HEAD_DIM + 16, rows + 2 * SPAN), BF16),
@@ -598,7 +788,10 @@
                 pltpu.VMEM((heads, 1, rows), F32),
                 pltpu.VMEM((rows, heads * HEAD_DIM), BF16),
                 pltpu.VMEM((rows, width), F32),
-                dma((7,)),
+                dma((9,)),
+                dma((2 * sp_n - 1,)),
+                dma((2 * tp_n - 1,)),
+                dma((2 + sp_n,)),
                 dma((sp_n - 1,)),
                 dma((sp_n,)),
                 dma((tp_n - 1,)),
@@ -606,7 +799,7 @@
                 dma((sp_n - 1,)),
                 dma((sp_n,)),
                 dma(((sp_n - 1) * (tp_n - 1),)),
-                dma((sp_n * tp_n,)),
+                dma(((sp_n - 1) * (tp_n - 1),)),
                 dma((2,)),
                 dma((2,)),
             ],

time: 35 us -> 30.7 us (0.88)
  Pallas kernels: 33.9 us -> 29.6 us
    pallas_call x1, Pallas kernels: 33.9 us -> 29.6 us  [shards(): pl.pallas_call(functools.partial(kernel, sp_n, tp_n), out_shape=jax.Shape...]
where the time goes in v2:
time: 30.7 us; the launch traced here: 30.5 us
  Pallas kernels  29.6 us (96%)
  local copies, waits for them, and re-layouts  0.97 us (3%)
    pallas_call x1, Pallas kernels, shards(): pl.pallas_call(functools.partial(kernel, sp_n, tp_n), out_shape=jax.Shape...  29.6 us
    unnamed x1, local copies, waits for them, and re-layouts  0.97 us

profile of v2, /device:TPU:0, one launch (start us, length us, event | category | flops | bytes accessed | tf_op | source)
XLA Modules:
  0.0 30.5 jit_solution(12090302754378524799)
XLA Ops:
  0.0 29.6 %shard_map.118 = bf16[256,2048]{1,0:T(8,128)(2,1)S(1)} custom-call(bf16[256,2048]{1,0:T(8,128)(2,1)} %latent_hbm.1, bf16[16,128]{1,0:T(8,128)(2,1)} %bitcast.6, bf16[256,2048]{1,0:T(8,128)(2,1)} %ctx_hbm.1, bf16[16,128]{1,0:T(8,128)(2,1)} %bitcast.7, bf16[3,512,512]{2,1,0:T(8,128)(2,1)} %mod_hbm.1, f32[1,2048]{1,0:T(1,128)} %bitcast.4, f32[1,2048]{1,0:T(1,128)} %bitcast.5, ...), custom_call_target="tpu_custom_call" | custom-call | tf_op jit(solution)/shard_map/pallas_call | solution.py:749
  29.6 1.0 %copy.14 = bf16[256,2048]{1,0:T(8,128)(2,1)} copy(bf16[256,2048]{1,0:T(8,128)(2,1)S(1)} %shard_map.118) | data formatting | bytes 2097152

commit v3 on v2

--- a/solution.py
+++ b/solution.py
@@ -221,8 +221,8 @@
         return pltpu.make_async_remote_copy(
             src_ref=gate_parts.at[sp],
             dst_ref=gate_parts.at[slot],
-            send_sem=gate_sem.at[step - 1],
-            recv_sem=gate_sem.at[sp_n - 1 + slot],
+            send_sem=z_send.at[step - 1],
+            recv_sem=gate_sem.at[slot],
             device_id={"sp": lax.rem(sp + step, sp_n), "tp": tp},
             device_id_type=MESH,
         )
@@ -231,8 +231,8 @@
         return pltpu.make_async_remote_copy(
             src_ref=gates.at[tp],
             dst_ref=gates.at[slot],
-            send_sem=gate_gat_sem.at[step - 1],
-            recv_sem=gate_gat_sem.at[tp_n - 1 + slot],
+            send_sem=gat_send.at[step - 1],
+            recv_sem=gate_gat_sem.at[slot],
             device_id={"sp": sp, "tp": lax.rem(tp + step, tp_n)},
             device_id_type=MESH,
         )
@@ -261,7 +261,7 @@
         return pltpu.make_async_remote_copy(
             src_ref=vecs.at[tp],
             dst_ref=vecs.at[slot],
-            send_sem=gat_send.at[step - 1],
+            send_sem=f_send.at[step - 1],
             recv_sem=gat_recv.at[slot],
             device_id={"sp": sp, "tp": partner(step)},
             device_id_type=MESH,
@@ -334,6 +334,8 @@
         term = dot(ctx_hidden[pl.ds(first, quarter), features], wkv[features])
         total = term if total is None else total + term
     ctx_kv[ctx_rows_of(tp)] = total.astype(BF16)
+    for step in range(1, sp_n):
+        sum_copy(step, sp).wait_send()
 
     def peer(step):
         if rich:
@@ -347,7 +349,7 @@
         return pltpu.make_async_remote_copy(
             src_ref=share(s, tp),
             dst_ref=share(s, tp),
-            send_sem=z_send.at[step - 1],
+            send_sem=sum_send.at[step - 1],
             recv_sem=z_recv.at[s],
             device_id={"sp": peer(step), "tp": tp},
             device_id_type=MESH,
@@ -499,6 +501,8 @@
                 q_rot[i, base + half : base + HEAD_DIM, side] = r2[:, b * SPAN : (b + 1) * SPAN]
 
     for step in range(1, tp_n):
+        gat_copy(step, tp).wait_send()
+    for step in range(1, tp_n):
         for t in range(tp_n):
             modulate(ctx, ctx_hidden, 1, pl.multiple_of(partner(step) * quarter, 16), quarter, t)
     mine[...] = dot(ctx_hidden[...], wkv[...]).astype(BF16)
@@ -706,11 +710,9 @@
         out_ref[:, at] = (latent[:, at].astype(F32) + projected[:, at] * r * gain).astype(BF16)
 
     for step in range(1, sp_n):
-        sum_copy(step, sp).wait_send()
         gate_sum_copy(step, sp).wait_send()
         z_copy(step, sp).wait_send()
     for step in range(1, tp_n):
-        gat_copy(step, tp).wait_send()
         gate_copy(step, tp).wait_send()
         for far in range(1, sp_n):
             done = f_copy(far, step, peer(far), tp)
@@ -789,8 +791,8 @@
                 pltpu.VMEM((rows, heads * HEAD_DIM), BF16),
                 pltpu.VMEM((rows, width), F32),
                 dma((9,)),
-                dma((2 * sp_n - 1,)),
-                dma((2 * tp_n - 1,)),
+                dma((sp_n,)),
+                dma((tp_n,)),
                 dma((2 + sp_n,)),
                 dma((sp_n - 1,)),
                 dma((sp_n,)),

time: 30.7 us -> 30.7 us (level)
  no operation moved by 1% of the time
where the time goes in v3:
time: 30.7 us; the launch traced here: 30.5 us
  Pallas kernels  29.5 us (96%)
  local copies, waits for them, and re-layouts  0.97 us (3%)
    pallas_call x1, Pallas kernels, shards(): pl.pallas_call(functools.partial(kernel, sp_n, tp_n), out_shape=jax.Shape...  29.5 us
    unnamed x1, local copies, waits for them, and re-layouts  0.97 us

profile of v3, /device:TPU:0, one launch (start us, length us, event | category | flops | bytes accessed | tf_op | source)
XLA Modules:
  0.0 30.5 jit_solution(12437406342027616633)
XLA Ops:
  0.0 29.5 %shard_map.118 = bf16[256,2048]{1,0:T(8,128)(2,1)S(1)} custom-call(bf16[256,2048]{1,0:T(8,128)(2,1)} %latent_hbm.1, bf16[16,128]{1,0:T(8,128)(2,1)} %bitcast.6, bf16[256,2048]{1,0:T(8,128)(2,1)} %ctx_hbm.1, bf16[16,128]{1,0:T(8,128)(2,1)} %bitcast.7, bf16[3,512,512]{2,1,0:T(8,128)(2,1)} %mod_hbm.1, f32[1,2048]{1,0:T(1,128)} %bitcast.4, f32[1,2048]{1,0:T(1,128)} %bitcast.5, ...), custom_call_target="tpu_custom_call" | custom-call | tf_op jit(solution)/shard_map/pallas_call | solution.py:751
  29.5 1.0 %copy.14 = bf16[256,2048]{1,0:T(8,128)(2,1)} copy(bf16[256,2048]{1,0:T(8,128)(2,1)S(1)} %shard_map.118) | data formatting | bytes 2097152
